TPU v7x, 32 devices: a whole 2x2x4 slice. The times are simulated.
32 devices in a mesh: sp: 4 (over z), fs: 4 (over y, x), tp: 2 (over core).
Axes of the slice: x: 2, y: 2, z: 4, core: 2. Of those that a mesh axis runs over, the one named last changes fastest.
Arguments:
- tokens: bfloat16 [2048, 2048], P(('fs', 'sp'), 'tp'), parts along dimension 0, may hold values from -6 to 6
- norm_gain: float32 [2048], replicated, may hold values from 0.1 to 1.9
- w_recur_in: bfloat16 [2048, 1024], P(None, 'tp'), may hold values from -0.125 to 0.125
- conv_weight: float32 [4, 1024], P(None, 'tp'), may hold values from -3 to 3
- w_gate_decay: bfloat16 [16, 64, 64], P('tp'), may hold values from -0.75 to 0.75
- w_gate_input: bfloat16 [16, 64, 64], P('tp'), may hold values from -0.75 to 0.75
- decay_base: float32 [1024], P('tp'), may hold values from 0 to 0.01, as said below
- extra_decay: float32 [2048, 16], P(('fs', 'sp'), 'tp'), parts along dimension 0, may hold values from 0 to 1, as said below
- w_query: bfloat16 [2048, 1024], P(None, 'tp'), may hold values from -1 to 1
- w_key: bfloat16 [2048, 256], P(None, 'tp'), may hold values from -20 to 20
- w_value: bfloat16 [2048, 256], P(None, 'tp'), may hold values from -0.125 to 0.125
- mix_lambda: float32 [8], P('tp'), may hold values from 0.3 to 0.8
- head_gain: float32 [128], replicated, may hold values from 0.1 to 1.9
- w_out_recur: bfloat16 [1024, 2048], P('tp'), may hold values from -0.125 to 0.125
- w_out_attend: bfloat16 [1024, 2048], P('tp'), may hold values from -0.125 to 0.125
- out_gain: float32 [2048], replicated, may hold values from 0.1 to 1.9
Outputs:
- mixed: bfloat16 [2048, 2048], P(('fs', 'sp', 'tp')), parts along dimension 0
There are 4 independent parts, one for each index of `fs`. A program takes and returns all parts, laid end to end along the dimension named above; an argument that names none is the same for every part. Nothing has to cross between parts.
Inputs may be any that keep to these rules, and one draw needn't show every extreme that they name: `decay_base`: positive rates of each channel. `extra_decay`: non-negative added log-decays.
All inputs are finite; a program needn't handle non-finite values.
Results may differ from a plain program's by a relative error of at most 0.012.
The roundings to bfloat16 on the way count: a program that leaves them out, or rounds other values in their place, can miss the bound.
Values may be sent and summed in bfloat16 or wider, within the bound.
A program may use at most 128 MiB of HBM per device.

v0:
```python
import jax
import jax.numpy as jnp
from jax import lax
from jax.sharding import PartitionSpec as P

D = 2048
HEAD = 64
DV = 128


lru_rate = 8.0
norm_eps = 1e-06


def shifted(block, axis, distance):
    devices = range(lax.axis_size(axis))
    route = [(i - distance, i) for i in devices if i - distance in devices]
    return lax.ppermute(block, axis, route)


def prefix(part, axis, combine, identity):
    place = lax.axis_index(axis)
    gathered = jax.tree.map(lambda a: lax.all_gather(a, axis), part)
    state = jax.tree.map(lambda a, e: jnp.zeros_like(a) + jnp.asarray(e, a.dtype), part, identity)

    def one(lap, state):
        return combine(
            state, jax.tree.map(lambda a: lax.dynamic_index_in_dim(a, lap, 0, False), gathered)
        )

    return lax.fori_loop(0, place, one, state)


def chain(earlier, later):
    return (earlier[0] * later[0], later[0] * earlier[1] + later[1])


def body(
    tokens,
    norm_gain,
    w_recur_in,
    conv_weight,
    w_gate_decay,
    w_gate_input,
    decay_base,
    extra_decay,
    w_query,
    w_key,
    w_value,
    mix_lambda,
    head_gain,
    w_out_recur,
    w_out_attend,
    out_gain,
):
    row_count = tokens.shape[0]
    recur_cols = w_recur_in.shape[1]
    query_cols = w_query.shape[1]
    key_cols = w_key.shape[1]
    all_weights = jnp.concatenate([w_recur_in, w_query, w_key, w_value], axis=1)
    wide_piece = lax.all_gather(tokens, "tp", axis=1, tiled=True).astype(jnp.float32)
    scaled = (wide_piece * norm_gain).astype(jnp.bfloat16)
    accum = jnp.dot(scaled, all_weights, preferred_element_type=jnp.float32)
    squares = jnp.sum(wide_piece * wide_piece, axis=1, keepdims=True)
    accum, squares = (accum, squares)
    inverse = lax.rsqrt(squares / D + norm_eps)
    projected = (accum * inverse).astype(jnp.bfloat16)
    recur_in = projected[:, :recur_cols]
    queries = projected[:, recur_cols : recur_cols + query_cols]
    keys = projected[:, recur_cols + query_cols : recur_cols + query_cols + key_cols]
    values = projected[:, recur_cols + query_cols + key_cols :]
    taps = conv_weight.shape[0]
    carried_rows = shifted(recur_in[row_count - (taps - 1) :], "sp", 1)
    padded = jnp.concatenate([carried_rows, recur_in], axis=0).astype(jnp.float32)
    conv_acc = jnp.zeros((row_count, recur_cols), jnp.float32)
    for offset in range(taps):
        conv_acc = conv_acc + conv_weight[offset] * padded[offset : offset + row_count]
    conv_in = conv_acc.astype(jnp.bfloat16)
    gate_blocks = w_gate_decay.shape[0]
    blocks = conv_in.reshape(row_count, gate_blocks, HEAD)
    decay_gate = jax.nn.sigmoid(
        jnp.einsum("thi,hij->thj", blocks, w_gate_decay, preferred_element_type=jnp.float32)
    ).reshape(row_count, recur_cols)
    input_gate = jax.nn.sigmoid(
        jnp.einsum("thi,hij->thj", blocks, w_gate_input, preferred_element_type=jnp.float32)
    ).reshape(row_count, recur_cols)
    log_decay = -lru_rate * decay_gate * decay_base - jnp.repeat(extra_decay, HEAD, axis=1)
    decay = jnp.exp(log_decay)
    inject = jnp.sqrt(-jnp.expm1(2.0 * log_decay)) * input_gate * conv_in.astype(jnp.float32)
    decay_cum, local_state = lax.associative_scan(chain, (decay, inject), axis=0)
    identity = (jnp.ones((recur_cols,), jnp.float32), jnp.zeros((recur_cols,), jnp.float32))
    carried = prefix((decay_cum[row_count - 1], local_state[row_count - 1]), "sp", chain, identity)
    recur_out = (local_state + decay_cum * carried[1]).astype(jnp.bfloat16)
    kv_local = key_cols // (2 * HEAD)
    heads_local = query_cols // (2 * HEAD)
    group_size = heads_local // kv_local
    local_query = queries.reshape(row_count, kv_local, group_size, 2, HEAD)
    offset_rows = lax.axis_index("sp") * row_count
    positions = offset_rows + jnp.arange(row_count, dtype=jnp.int32)
    last_position = offset_rows + row_count - 1
    lambdas = mix_lambda.reshape(kv_local, group_size)
    start_state = (
        jnp.full((2, kv_local, group_size, row_count), -1e30, jnp.float32),
        jnp.zeros((2, kv_local, group_size, row_count), jnp.float32),
        jnp.zeros((2, row_count, kv_local, group_size, DV), jnp.float32),
    )
    key_piece = lax.all_gather(keys, "sp", axis=0, tiled=True)
    value_piece = lax.all_gather(values, "sp", axis=0, tiled=True)
    count = key_piece.shape[0]

    def update(state):
        peaks, totals, attends = state
        key_three = key_piece.reshape(count, kv_local, 2, HEAD)
        value_three = value_piece.reshape(count, kv_local, DV)
        allowed = positions[:, None] >= jnp.arange(count, dtype=jnp.int32)[None, :]
        new_peaks, new_totals, new_attends = ([], [], [])
        for mapping in range(2):
            scores = jnp.einsum(
                "bkgd,tkd->kgbt",
                local_query[:, :, :, mapping, :],
                key_three[:, :, mapping, :],
                preferred_element_type=jnp.float32,
            ) * HEAD ** (-0.5)
            scores = jnp.where(allowed, scores, -jnp.inf)
            peak = jnp.maximum(peaks[mapping], jnp.max(scores, axis=-1))
            correction = jnp.exp(peaks[mapping] - peak)
            expo = jnp.exp(scores - peak[..., None])
            new_totals.append(totals[mapping] * correction + jnp.sum(expo, axis=-1))
            gained = jnp.einsum(
                "kgbt,tke->bkge",
                expo.astype(jnp.bfloat16),
                value_three,
                preferred_element_type=jnp.float32,
            )
            new_attends.append(
                attends[mapping] * jnp.transpose(correction, (2, 0, 1))[..., None] + gained
            )
            new_peaks.append(peak)
        return (jnp.stack(new_peaks), jnp.stack(new_totals), jnp.stack(new_attends))

    peaks, totals, attends = lax.cond(
        jnp.int32(0) <= last_position, update, lambda state: state, start_state
    )
    first = attends[0] / jnp.transpose(totals[0], (2, 0, 1))[..., None]
    second = attends[1] / jnp.transpose(totals[1], (2, 0, 1))[..., None]
    head_out = (first - lambdas[None, :, :, None] * second).reshape(row_count, heads_local, DV)
    normed = (
        head_out
        * lax.rsqrt(jnp.mean(head_out * head_out, axis=-1, keepdims=True) + norm_eps)
        * head_gain
    )
    attend_out = normed.astype(jnp.bfloat16).reshape(row_count, heads_local * DV)
    recur_rows, attend_rows = (
        lax.all_to_all(recur_out, "tp", split_axis=0, concat_axis=1, tiled=True),
        lax.all_to_all(attend_out, "tp", split_axis=0, concat_axis=1, tiled=True),
    )
    whole_recur, whole_attend = (
        lax.all_gather(w_out_recur, "tp", axis=0, tiled=True),
        lax.all_gather(w_out_attend, "tp", axis=0, tiled=True),
    )
    merged = jnp.dot(recur_rows, whole_recur, preferred_element_type=jnp.float32) + jnp.dot(
        attend_rows, whole_attend, preferred_element_type=jnp.float32
    )
    final = (
        merged * lax.rsqrt(jnp.mean(merged * merged, axis=1, keepdims=True) + norm_eps) * out_gain
    )
    return final.astype(jnp.bfloat16)


def solution(mesh):
    in_specs = (
        P(("fs", "sp"), "tp"),
        P(),
        P(None, "tp"),
        P(None, "tp"),
        P("tp", None, None),
        P("tp", None, None),
        P("tp"),
        P(("fs", "sp"), "tp"),
        P(None, "tp"),
        P(None, "tp"),
        P(None, "tp"),
        P("tp"),
        P(),
        P("tp", None),
        P("tp", None),
        P(),
    )
    out_specs = P(("fs", "sp", "tp"), None)
    return jax.shard_map(body, mesh=mesh, in_specs=in_specs, out_specs=out_specs, check_vma=False)
```

profile of v0, /device:TPU:0, one launch (start us, length us, event | category | flops | bytes accessed | tf_op | source)
XLA Modules:
  0.0 101.6 jit_solution(12139623973826426824)
XLA Ops:
  6.5 0.7 all-gather.5.cloned.1.call-update
  7.3 2.5 %all_gather.21 = bf16[128,2048]{1,0:T(8,128)(2,1)S(1)} all-gather(bf16[128,1024]{1,0:T(8,128)(2,1)} %param.20), channel_id=1, replica_groups=mesh['sp'=4,'fs'=4,'tp'=2] {'tp'}, dimensions={1}, use_global_device_ids=true | all-gather | bytes 786432 | tf_op jit(solution)/shard_map/all_gather | solution.py:61
  9.8 0.2 fusion.43
  10.0 3.2 %fusion.33 = bf16[128,1280]{1,0:T(8,128)(2,1)S(1)} fusion(bf16[2048,128]{1,0:T(8,128)(2,1)} %param.30, bf16[2048,128]{1,0:T(8,128)(2,1)} %param.29, bf16[2048,512]{1,0:T(8,128)(2,1)} %param.28, bf16[2048,512]{1,0:T(8,128)(2,1)} %param.22, bf16[128,2048]{1,0:T(8,128)(2,1)S(1)} %all_gather.21, f32[2048]{0:T(1024)} %param.21, f32[128]{0:T(128)S(1)} %add_rsqrt_fusion.2), kind=kOutput, calls=%fused_computation.52 | convolution fusion | flops 693174272 | bytes 6103552 | tf_op jit(solution)/shard_map/dot_general | solution.py:63
  13.2 4.8 %collective-permute-start = (bf16[3,512]{1,0:T(4,128)(2,1)S(1)}, bf16[3,512]{1,0:T(4,128)(2,1)S(1)}, u32[]{:S(2)}, u32[]{:S(2)}) collective-permute-start(bf16[3,512]{1,0:T(4,128)(2,1)S(1)} %slice.358), channel_id=1, source_target_pairs={{0,8},{8,16},{16,24},{1,9},{9,17},{17,25},{2,10},{10,18},{18,26},{... | collective-permute-start | bytes 9224 | tf_op jit(solution)/shard_map/ppermute | solution.py:18
  18.0 13.6 %all_gather.25 = bf16[512,128]{1,0:T(8,128)(2,1)S(1)} all-gather(bf16[128,128]{1,0:T(8,128)(2,1)S(1)} %get-tuple-element.115), channel_id=1, replica_groups=mesh['sp'=4,'fs'=4,'tp'=2] {'sp'}, dimensions={0}, use_global_device_ids=true | all-gather | bytes 163840 | tf_op jit(solution)/shard_map/all_gather | solution.py:107
  31.6 13.4 %all_gather.26 = bf16[512,128]{1,0:T(8,128)(2,1)S(1)} all-gather(bf16[128,128]{1,0:T(8,128)(2,1)S(1)} %get-tuple-element.114), channel_id=1, replica_groups=mesh['sp'=4,'fs'=4,'tp'=2] {'sp'}, dimensions={0}, use_global_device_ids=true | all-gather | bytes 163840 | tf_op jit(solution)/shard_map/all_gather | solution.py:108
  45.0 2.2 %conditional.1 = (f32[2,1,4,128]{3,2,1,0:T(4,128)S(1)}, f32[2,128,1,4,128]{4,1,3,2,0:T(8,128)S(1)}) conditional(s32[]{:T(128)} %convert_element_type.45, () %tuple.21, (s32[]{:T(128)}, s32[128]{0:T(128)S(1)}, bf16[512,128]{1,0:T(8,128)(2,1)S(1)}, bf16[128,1280]{1,0:T(8,128)(2,1)S(1)}, bf16[512,128]{1,0:T(8,128)(2,1)S(1)}) %tuple.22), branch_computations={%region_3.4_spmd, %region_4.9_spmd} | conditional | flops 205328512 | bytes 9819668 | solution.py:141
  45.0 0.2 copy.57
  45.3 0.1 copy.56
  45.4 0.3 fusion.65
  45.8 0.2 fusion.11
  46.0 0.3 fusion.66
  46.3 0.2 fusion.9
  46.5 0.4 fusion.5
  46.9 0.4 fusion.7
  47.3 0.1 copy.72
  47.4 0.1 copy.73
  47.5 0.3 fusion.53
  47.9 0.1 copy.62
  48.0 0.2 mul.337
  48.2 0.1 mul.338
  48.4 0.2 copy.58
  48.7 0.2 copy.60
  49.0 0.2 div.75.clone
  49.2 0.1 div.76
  49.3 0.2 div.79.clone
  49.5 0.1 div.80
  49.7 0.8 multiply_convert_fusion.1
  50.5 3.4 %all-to-all-start.1 = ((bf16[2,64,512]{2,1,0:T(8,128)(2,1)}), bf16[2,64,512]{2,1,0:T(8,128)(2,1)S(1)}, u32[]{:S(2)}, u32[]{:S(2)}) async-start(bf16[2,64,512]{2,1,0:T(8,128)(2,1)} %multiply_convert_fusion.1), calls=%async_computation.1 | async-start | bytes 262144 | tf_op jit(solution)/shard_map/all_to_all | solution.py:155
  53.9 0.7 all-gather.7.cloned.1.call-update
  54.7 0.1 copy.52
  54.8 0.5 all-to-all-done.1
  55.4 0.1 fusion.47
  55.5 0.1 copy.49
  55.6 0.3 fusion.41
  55.9 0.1 copy.51
  56.0 0.3 fusion.38
  56.3 0.1 copy.54
  56.5 0.3 convert_multiply_fusion.2
  58.2 0.2 slice.282
  58.4 0.2 slice.331
  59.6 11.9 %all-gather.1 = f32[4,1,512]{2,1,0:T(1,128)S(1)} all-gather(f32[1,1,512]{2,1,0:T(1,128)S(1)} %add_bitcast_fusion.2), channel_id=1, replica_groups=mesh['sp'=4,'fs'=4,'tp'=2] {'sp'}, dimensions={0}, use_global_device_ids=true | all-gather | bytes 10240 | tf_op jit(solution)/shard_map/all_gather | solution.py:23
  71.7 11.9 %all-gather = f32[4,1,512]{2,1,0:T(1,128)S(1)} all-gather(f32[1,1,512]{2,1,0:T(1,128)S(1)} %add_bitcast_fusion.3), channel_id=1, replica_groups=mesh['sp'=4,'fs'=4,'tp'=2] {'sp'}, dimensions={0}, use_global_device_ids=true | all-gather | bytes 10240 | tf_op jit(solution)/shard_map/all_gather | solution.py:23
  83.8 3.8 %all_to_all.35 = bf16[2,64,512]{2,1,0:T(8,128)(2,1)S(1)} all-to-all(bf16[2,64,512]{2,1,0:T(8,128)(2,1)S(1)} %bitcast.174), channel_id=1, replica_groups=mesh['sp'=4,'fs'=4,'tp'=2] {'tp'}, dimensions={0} | all-to-all | bytes 262144 | tf_op jit(solution)/shard_map/all_to_all | solution.py:154
  87.6 3.0 %fusion.71 = f32[64,2048]{1,0:T(8,128)S(1)} fusion(bf16[64,1024]{1,0:T(8,128)(2,1)S(1)} %bitcast.175, bf16[1024,2048]{1,0:T(8,128)(2,1)} %all-gather.5.cloned.1.call-done), kind=kOutput, calls=%fused_computation.154 | convolution fusion | flops 268435456 | bytes 4849664 | tf_op jit(solution)/shard_map/dot_general | solution.py:161
  90.7 3.2 %multiply_reduce_fusion = (f32[64]{0:T(128)S(1)}, f32[64,2048]{1,0:T(8,128)S(1)}) fusion(f32[64,2048]{1,0:T(8,128)S(1)} %fusion.71, bf16[64,1024]{1,0:T(8,128)(2,1)S(1)} %bitcast.173, bf16[1024,2048]{1,0:T(8,128)(2,1)} %all-gather.7.cloned.1.call-done), kind=kOutput, calls=%fused_computation.67 | convolution fusion | flops 268828608 | bytes 5374208 | tf_op jit(solution)/shard_map/dot_general | solution.py:161
  93.9 0.8 multiply_convert_fusion
  (155 shorter events, 2.8 us)
Async XLA Ops:
  6.5 49.1 %copy-start = (bf16[8,64,64]{2,1,0:T(8,128)(2,1)S(1)}, bf16[8,64,64]{2,1,0:T(8,128)(2,1)}, u32[]{:S(2)}) copy-start(bf16[8,64,64]{2,1,0:T(8,128)(2,1)} %param.24) | copy-start | bytes 196612
  6.5 81.1 %all-gather.5.cloned.1.call-start = ((), (), s32[]{:S(2)}) async-start(), calls=%async_computation.2 | async-start | bytes 6291456 | tf_op jit(solution)/shard_map/all_gather | solution.py:158
  13.2 42.1 %collective-permute-start = (bf16[3,512]{1,0:T(4,128)(2,1)S(1)}, bf16[3,512]{1,0:T(4,128)(2,1)S(1)}, u32[]{:S(2)}, u32[]{:S(2)}) collective-permute-start(bf16[3,512]{1,0:T(4,128)(2,1)S(1)} %slice.358), channel_id=1, source_target_pairs={{0,8},{8,16},{16,24},{1,9},{9,17},{17,25},{2,10},{10,18},{18,26},{... | collective-permute-start | bytes 9224 | tf_op jit(solution)/shard_map/ppermute | solution.py:18
  45.0 2.5 %copy-start.4 = (f32[4]{0:T(128)S(1)}, f32[4]{0:T(128)}, u32[]{:S(2)}) copy-start(f32[4]{0:T(128)} %param.31) | copy-start | bytes 52
  47.3 2.3 %copy-start.6 = (f32[128]{0:T(128)S(1)}, f32[128]{0:T(128)}, u32[]{:S(2)}) copy-start(f32[128]{0:T(128)} %param.32) | copy-start | bytes 1540
  48.3 6.3 %copy-start.2 = (f32[4,512]{1,0:T(4,128)S(1)}, f32[4,512]{1,0:T(4,128)}, u32[]{:S(2)}) copy-start(f32[4,512]{1,0:T(4,128)} %param.23) | copy-start | bytes 24580
  48.3 6.3 %copy-start.5 = (f32[512]{0:T(512)S(1)}, f32[512]{0:T(512)}, u32[]{:S(2)}) copy-start(f32[512]{0:T(512)} %param.26) | copy-start | bytes 6148
  48.4 6.3 %copy-start.3 = (f32[128,8]{0,1:T(8,128)S(1)}, f32[128,8]{0,1:T(8,128)}, u32[]{:S(2)}) copy-start(f32[128,8]{0,1:T(8,128)} %param.27) | copy-start | bytes 12292
  49.7 6.4 %copy-start.7 = (bf16[8,64,64]{2,1,0:T(8,128)(2,1)S(1)}, bf16[8,64,64]{2,1,0:T(8,128)(2,1)}, u32[]{:S(2)}) copy-start(bf16[8,64,64]{2,1,0:T(8,128)(2,1)} %param.25) | copy-start | bytes 196612
  50.5 4.8 %all-to-all-start.1 = ((bf16[2,64,512]{2,1,0:T(8,128)(2,1)}), bf16[2,64,512]{2,1,0:T(8,128)(2,1)S(1)}, u32[]{:S(2)}, u32[]{:S(2)}) async-start(bf16[2,64,512]{2,1,0:T(8,128)(2,1)} %multiply_convert_fusion.1), calls=%async_computation.1 | async-start | bytes 262144 | tf_op jit(solution)/shard_map/all_to_all | solution.py:155
  53.8 36.9 %all-gather.7.cloned.1.call-start = ((), (), s32[]{:S(2)}) async-start(), calls=%async_computation.3 | async-start | bytes 6291456 | tf_op jit(solution)/shard_map/all_gather | solution.py:159
  87.6 6.3 %copy-start.1 = (f32[2048]{0:T(1024)S(1)}, f32[2048]{0:T(1024)}, u32[]{:S(2)}) copy-start(f32[2048]{0:T(1024)} %param.35) | copy-start | bytes 24580
Sparse Core Ops, SparseCore 0:
  8.9 16.3 all-gather.4
  56.2 12.8 all-gather.6
where the time goes:
time: 102 us
  blocking collectives  57.2 us (56%)
  between operations  14.4 us (14%)
  matrix products  11.3 us (11%)
  starting transfers between devices  8.26 us (8%)
  local copies, waits for them, and re-layouts  4.75 us (5%)
  other arithmetic  3.69 us (4%)
  waiting for transfers between devices  1.91 us (2%)
    all_gather x2, blocking collectives, prefix(): gathered = jax.tree.map(lambda a: lax.all_gather(a, axis), part)  23.9 us
    all_gather x1, blocking collectives, body(): key_piece = lax.all_gather(keys, 'sp', axis=0, tiled=True)  13.6 us
    all_gather x1, blocking collectives, body(): value_piece = lax.all_gather(values, 'sp', axis=0, tiled=True)  13.4 us
    ppermute x1, starting transfers between devices, shifted(): return lax.ppermute(block, axis, route)  4.84 us
    all_to_all x1, blocking collectives, body(): lax.all_to_all(recur_out, 'tp', split_axis=0, concat_axis=1, tiled=True)  3.84 us
    all_to_all x1, starting transfers between devices, body(): lax.all_to_all(attend_out, 'tp', split_axis=0, concat_axis=1, tiled=True)  3.38 us
    dot_general x1, matrix products, body(): accum = jnp.dot(scaled, all_weights, preferred_element_type=jnp.float32)  3.19 us
    dot_general x1, matrix products, body(): jnp.dot(attend_rows, whole_attend, preferred_element_type=jnp.float32)  3.16 us
  transfers between devices with their start and end apart: 4, of which 1 were waited for; matrix products, arithmetic and copies ran while one was open for 15% of the time, Pallas kernels for 0%

commit v1 on v0

v1 whole, which is shorter than its diff:
```python
import functools

import jax
import jax.numpy as jnp
from jax import lax
from jax.experimental import pallas as pl
from jax.experimental.pallas import tpu as pltpu
from jax.sharding import PartitionSpec as P

HEAD = 64
PAIR = 2 * HEAD
MESH = pl.DeviceIdType.MESH
F32 = jnp.float32
BF16 = jnp.bfloat16

lru_rate = 8.0
norm_eps = 1e-06


def dot(a, b):
    return jnp.dot(a, b, preferred_element_type=F32)


def minus_expm1(y):
    series = 1.0 + y * (1.0 / 6.0)
    for k in (5.0, 4.0, 3.0, 2.0):
        series = 1.0 + y * (1.0 / k) * series
    return jnp.where(y > -0.25, -y * series, 1.0 - jnp.exp(y))


def kernel(
    sp_size,
    tp_size,
    taps,
    tokens,
    norm_gain,
    w_recur_in,
    conv_weight,
    w_gate_decay,
    w_gate_input,
    decay_base,
    extra_decay,
    w_query,
    w_key,
    w_value,
    mix_lambda,
    head_gain,
    w_out_recur,
    w_out_attend,
    out_gain,
    out,
    tok,
    scaled,
    wkv,
    wr,
    wq,
    wor,
    woa,
    v_norm_gain,
    v_conv,
    v_gate_decay,
    v_gate_input,
    v_base,
    v_extra,
    v_head_gain,
    v_out_gain,
    gates,
    acc_kv,
    acc_r,
    acc_q,
    kv,
    rbuf,
    qbuf,
    peaks,
    totals,
    attends,
    cum_decay,
    local_state,
    carry_out,
    carry_in,
    carried,
    attend_out,
    merged,
    part_out,
    part_in,
    load_sem,
    tok_sem,
    kv_send,
    kv_recv,
    halo_sem,
    carry_send,
    carry_recv,
    part_send,
    part_recv,
):
    me = lax.axis_index("sp")
    core = lax.axis_index("tp")
    partner = 1 - core
    rows, half = tokens.shape
    width = half * tp_size
    recur_cols = wr.shape[1]
    key_cols = w_key.shape[1]
    query_cols = wq.shape[1]
    kv_local = key_cols // PAIR
    heads = query_cols // PAIR
    group = heads // kv_local
    halo = rbuf.shape[0] - rows
    own_rows = rows // tp_size
    chunks, _, chunk = part_out.shape

    barrier = pltpu.get_barrier_semaphore()
    pl.semaphore_signal(barrier, inc=1, device_id={"tp": partner}, device_id_type=MESH)
    for step in range(1, sp_size):
        other = lax.rem(me + step, sp_size)
        pl.semaphore_signal(barrier, inc=1, device_id={"sp": other}, device_id_type=MESH)

    mine = pl.ds(pl.multiple_of(core * half, half), half)
    theirs = pl.ds(pl.multiple_of(partner * half, half), half)
    plan = {}

    def load(name, src, dst):
        copy = pltpu.make_async_copy(src, dst, load_sem.at[len(plan)])
        copy.start()
        plan[name] = copy

    load("tok", tokens, tok.at[core])
    load("norm_gain", norm_gain, v_norm_gain)
    load("k0", w_key.at[mine], wkv.at[mine, pl.ds(0, key_cols)])
    load("v0", w_value.at[mine], wkv.at[mine, pl.ds(key_cols, wkv.shape[1] - key_cols)])
    load("r0", w_recur_in.at[mine], wr.at[mine])
    load("q0", w_query.at[mine], wq.at[mine])
    load("k1", w_key.at[theirs], wkv.at[theirs, pl.ds(0, key_cols)])
    load("v1", w_value.at[theirs], wkv.at[theirs, pl.ds(key_cols, wkv.shape[1] - key_cols)])
    load("r1", w_recur_in.at[theirs], wr.at[theirs])
    load("q1", w_query.at[theirs], wq.at[theirs])
    load("gate_decay", w_gate_decay, v_gate_decay)
    load("gate_input", w_gate_input, v_gate_input)
    load("conv", conv_weight, v_conv)
    load("base", decay_base, v_base)
    load("extra", extra_decay, v_extra)
    load("head_gain", head_gain, v_head_gain)
    load("out_gain", out_gain, v_out_gain)
    load("wor", w_out_recur, wor)
    load("woa", w_out_attend, woa)

    pl.semaphore_wait(barrier, sp_size)
    tok_copy = pltpu.make_async_remote_copy(
        tokens, tok.at[core], tok_sem.at[0], tok_sem.at[1],
        device_id={"tp": partner}, device_id_type=MESH,
    )
    tok_copy.start()

    def scale(part, columns):
        wide = tok[part].astype(F32)
        scaled[part] = (wide * v_norm_gain[:, columns]).astype(BF16)
        return jnp.sum(wide * wide, axis=1, keepdims=True)

    plan["tok"].wait()
    plan["norm_gain"].wait()
    squares = scale(core, mine)
    own = scaled[core]
    plan["k0"].wait()
    plan["v0"].wait()
    acc_kv[...] = dot(own, wkv[mine, :])
    plan["r0"].wait()
    acc_r[...] = dot(own, wr[mine, :])
    plan["q0"].wait()
    acc_q[...] = dot(own, wq[mine, :])

    tok_copy.wait_recv()
    squares = squares + scale(partner, theirs)
    inverse = lax.rsqrt(squares / width + norm_eps)
    far = scaled[partner]
    plan["k1"].wait()
    plan["v1"].wait()
    kv[me] = ((acc_kv[...] + dot(far, wkv[theirs, :])) * inverse).astype(BF16)

    def kv_copy(step):
        return pltpu.make_async_remote_copy(
            kv.at[me], kv.at[me], kv_send.at[step], kv_recv.at[step],
            device_id={"sp": lax.rem(me + step, sp_size)}, device_id_type=MESH,
        )

    def kv_arrival(step):
        slot = kv.at[me - step]
        return pltpu.make_async_remote_copy(
            slot, slot, kv_send.at[step], kv_recv.at[step],
            device_id={"sp": lax.rem(me + step, sp_size)}, device_id_type=MESH,
        )

    for step in range(1, sp_size):
        @pl.when(me + step < sp_size)
        def _():
            kv_copy(step).start()

    plan["r1"].wait()
    rbuf[pl.ds(halo, rows), :] = ((acc_r[...] + dot(far, wr[theirs, :])) * inverse).astype(BF16)
    halo_copy = pltpu.make_async_remote_copy(
        rbuf.at[pl.ds(rows, halo)], rbuf.at[pl.ds(0, halo)], halo_sem.at[0], halo_sem.at[1],
        device_id={"sp": lax.rem(me + 1, sp_size)}, device_id_type=MESH,
    )

    @pl.when(me + 1 < sp_size)
    def _():
        halo_copy.start()

    @pl.when(me == 0)
    def _():
        rbuf[pl.ds(0, halo), :] = jnp.zeros((halo, recur_cols), BF16)

    plan["q1"].wait()
    query = (acc_q[...] + dot(far, wq[theirs, :])) * (inverse * HEAD ** (-0.5))
    for h in range(heads):
        qbuf[h] = query[:, h * PAIR : (h + 1) * PAIR].astype(BF16)

    lane = lax.broadcasted_iota(jnp.int32, (rows, PAIR), 1)
    row = lax.broadcasted_iota(jnp.int32, (rows, PAIR), 0)
    low = lane < HEAD

    def attend(block, first):
        for g in range(kv_local):
            keys = kv[block, :, g * PAIR : (g + 1) * PAIR].astype(F32)
            value = kv[block, :, key_cols + g * PAIR : key_cols + (g + 1) * PAIR]
            both = jnp.concatenate(
                [jnp.where(low, keys, 0.0).astype(BF16), jnp.where(low, 0.0, keys).astype(BF16)], 0
            )
            for h in range(g * group, (g + 1) * group):
                scores = lax.dot_general(
                    qbuf[h], both, (((1,), (1,)), ((), ())), preferred_element_type=F32
                )
                for m in range(2):
                    score = scores[:, m * rows : (m + 1) * rows]
                    if first:
                        score = jnp.where(row >= lane, score, -jnp.inf)
                    top = jnp.broadcast_to(jnp.max(score, axis=1, keepdims=True), score.shape)
                    if first:
                        peak = top
                        expo = jnp.exp(score - peak)
                        totals[h, m] = expo
                        attends[h, m] = dot(expo.astype(BF16), value)
                    else:
                        before = peaks[h, m]
                        peak = jnp.maximum(before, top)
                        fix = jnp.exp(before - peak)
                        expo = jnp.exp(score - peak)
                        totals[h, m] = totals[h, m] * fix + expo
                        attends[h, m] = attends[h, m] * fix + dot(expo.astype(BF16), value)
                    peaks[h, m] = peak

    attend(me, True)

    plan["gate_decay"].wait()
    plan["gate_input"].wait()
    blank = jnp.zeros((HEAD, HEAD), F32)
    pairs = gates.shape[0]
    for p in range(pairs):
        for column, source in enumerate((v_gate_decay, v_gate_input)):
            upper = jnp.concatenate([source[2 * p].astype(F32), blank], 1)
            lower = jnp.concatenate([blank, source[2 * p + 1].astype(F32)], 1)
            gates[p, :, column * PAIR : (column + 1) * PAIR] = jnp.concatenate(
                [upper, lower], 0
            ).astype(BF16)

    for name in ("conv", "base", "extra"):
        plan[name].wait()

    @pl.when(me > 0)
    def _():
        halo_copy.wait_recv()

    start = halo - (taps - 1)
    for p in range(pairs):
        columns = slice(p * PAIR, (p + 1) * PAIR)
        padded = rbuf[:, columns].astype(F32)
        conv = jnp.zeros((rows, PAIR), F32)
        for k in range(taps):
            conv = conv + v_conv[k : k + 1, columns] * padded[start + k : start + k + rows]
        conv_in = conv.astype(BF16)
        logits = dot(conv_in, gates[p])
        decay_gate = jax.nn.sigmoid(logits[:, :PAIR])
        input_gate = jax.nn.sigmoid(logits[:, PAIR:])
        extra = jnp.where(
            low,
            jnp.broadcast_to(v_extra[:, 2 * p : 2 * p + 1], (rows, PAIR)),
            jnp.broadcast_to(v_extra[:, 2 * p + 1 : 2 * p + 2], (rows, PAIR)),
        )
        log_decay = -lru_rate * decay_gate * v_base[:, columns] - extra
        decay = jnp.exp(log_decay)
        state = jnp.sqrt(minus_expm1(2.0 * log_decay)) * input_gate * conv_in.astype(F32)
        reach = 1
        while reach < rows:
            if reach < 8:
                earlier = row >= reach
                decay_before = jnp.where(earlier, pltpu.roll(decay, reach, 0), 1.0)
                state_before = jnp.where(earlier, pltpu.roll(state, reach, 0), 0.0)
            else:
                decay_before = jnp.concatenate(
                    [jnp.ones((reach, PAIR), F32), decay[: rows - reach]], 0
                )
                state_before = jnp.concatenate(
                    [jnp.zeros((reach, PAIR), F32), state[: rows - reach]], 0
                )
            state = decay * state_before + state
            decay = decay * decay_before
            reach *= 2
        cum_decay[:, columns] = decay
        local_state[:, columns] = state
        carry_out[0:1, columns] = decay[rows - 1 :]
        carry_out[1:2, columns] = state[rows - 1 :]

    def carry_copy(step, slot):
        return pltpu.make_async_remote_copy(
            carry_out, carry_in.at[slot], carry_send.at[step], carry_recv.at[step],
            device_id={"sp": lax.rem(me + step, sp_size)}, device_id_type=MESH,
        )

    for step in range(1, sp_size):
        @pl.when(me + step < sp_size)
        def _():
            carry_copy(step, me).start()

    def one(step, unused):
        kv_arrival(step).wait_recv()
        attend(me - step, False)
        return unused

    lax.fori_loop(1, me, one, 0)

    carried[...] = jnp.zeros_like(carried)

    def link(back, unused):
        step = me - back
        carry_copy(step, back).wait_recv()
        carried[...] = carry_in[back, 0:1] * carried[...] + carry_in[back, 1:2]
        return unused

    lax.fori_loop(0, me, link, 0)
    recur_out = (local_state[...] + cum_decay[...] * carried[...]).astype(BF16)
    plan["wor"].wait()
    for c in range(chunks):
        columns = slice(c * chunk, (c + 1) * chunk)
        merged[:, columns] = dot(recur_out, wor[:, columns])

    lax.fori_loop(jnp.maximum(me, 1), me + 1, one, 0)

    plan["head_gain"].wait()
    for h in range(heads):
        first, second = (
            attends[h, m] / jnp.sum(totals[h, m], axis=1, keepdims=True) for m in range(2)
        )
        head_out = first - mix_lambda[0, h] * second
        normed = (
            head_out
            * lax.rsqrt(jnp.mean(head_out * head_out, axis=1, keepdims=True) + norm_eps)
            * v_head_gain[...]
        )
        attend_out[:, h * PAIR : (h + 1) * PAIR] = normed.astype(BF16)

    plan["woa"].wait()
    attended = attend_out[...]

    def part_copy(c):
        return pltpu.make_async_remote_copy(
            part_out.at[c], part_in.at[c], part_send.at[c], part_recv.at[c],
            device_id={"tp": partner}, device_id_type=MESH,
        )

    keep = pl.ds(pl.multiple_of(core * own_rows, own_rows), own_rows)
    give = pl.ds(pl.multiple_of(partner * own_rows, own_rows), own_rows)
    for c in range(chunks):
        columns = slice(c * chunk, (c + 1) * chunk)
        merged[:, columns] = merged[:, columns] + dot(attended, woa[:, columns])
        part_out[c] = merged[give, columns].astype(BF16)
        part_copy(c).start()

    plan["out_gain"].wait()
    squares = jnp.zeros((own_rows, 1), F32)
    for c in range(chunks):
        columns = slice(c * chunk, (c + 1) * chunk)
        part_copy(c).wait_recv()
        whole = merged[keep, columns] + part_in[c].astype(F32)
        merged[keep, columns] = whole
        squares = squares + jnp.sum(whole * whole, axis=1, keepdims=True)
    final = lax.rsqrt(squares / out.shape[1] + norm_eps)
    for c in range(chunks):
        columns = slice(c * chunk, (c + 1) * chunk)
        out[:, columns] = (merged[keep, columns] * final * v_out_gain[:, columns]).astype(BF16)

    tok_copy.wait_send()
    for c in range(chunks):
        part_copy(c).wait_send()

    @pl.when(me + 1 < sp_size)
    def _():
        halo_copy.wait_send()

    for step in range(1, sp_size):
        @pl.when(me + step < sp_size)
        def _():
            kv_copy(step).wait_send()
            carry_copy(step, me).wait_send()


def body(sp_size, tp_size, *args):
    (tokens, norm_gain, w_recur_in, conv_weight, w_gate_decay, w_gate_input, decay_base,
     extra_decay, w_query, w_key, w_value, mix_lambda, head_gain, w_out_recur, w_out_attend,
     out_gain) = args
    rows, half = tokens.shape
    width = w_recur_in.shape[0]
    recur_cols, query_cols = w_recur_in.shape[1], w_query.shape[1]
    kv_cols = w_key.shape[1] + w_value.shape[1]
    heads = query_cols // PAIR
    pairs = recur_cols // PAIR
    out_width = w_out_recur.shape[1]
    chunk = min(512, out_width)
    chunks = out_width // chunk
    own_rows = rows // tp_size
    halo = 16
    line = lambda a: a.reshape(1, -1)
    operands = (tokens, line(norm_gain), w_recur_in, conv_weight, w_gate_decay, w_gate_input,
                line(decay_base), extra_decay, w_query, w_key, w_value, line(mix_lambda),
                line(head_gain), w_out_recur, w_out_attend, line(out_gain))
    anywhere = pl.BlockSpec(memory_space=pl.ANY)
    specs = [anywhere] * len(operands)
    specs[11] = pl.BlockSpec(memory_space=pltpu.SMEM)
    like = lambda a: pltpu.VMEM(a.shape, a.dtype)
    dma = lambda n: pltpu.SemaphoreType.DMA((n,))
    return pl.pallas_call(
        functools.partial(kernel, sp_size, tp_size, conv_weight.shape[0]),
        out_shape=jax.ShapeDtypeStruct((own_rows, out_width), BF16),
        in_specs=specs,
        out_specs=pl.BlockSpec(memory_space=pltpu.VMEM),
        scratch_shapes=[
            pltpu.VMEM((tp_size, rows, half), BF16),
            pltpu.VMEM((tp_size, rows, half), BF16),
            pltpu.VMEM((width, kv_cols), BF16),
            like(w_recur_in),
            like(w_query),
            like(w_out_recur),
            like(w_out_attend),
            like(operands[1]),
            like(conv_weight),
            like(w_gate_decay),
            like(w_gate_input),
            like(operands[6]),
            like(extra_decay),
            like(operands[12]),
            like(operands[15]),
            pltpu.VMEM((pairs, PAIR, 2 * PAIR), BF16),
            pltpu.VMEM((rows, kv_cols), F32),
            pltpu.VMEM((rows, recur_cols), F32),
            pltpu.VMEM((rows, query_cols), F32),
            pltpu.VMEM((sp_size, rows, kv_cols), BF16),
            pltpu.VMEM((halo + rows, recur_cols), BF16),
            pltpu.VMEM((heads, rows, PAIR), BF16),
            pltpu.VMEM((heads, 2, rows, PAIR), F32),
            pltpu.VMEM((heads, 2, rows, PAIR), F32),
            pltpu.VMEM((heads, 2, rows, PAIR), F32),
            pltpu.VMEM((rows, recur_cols), F32),
            pltpu.VMEM((rows, recur_cols), F32),
            pltpu.VMEM((2, recur_cols), F32),
            pltpu.VMEM((sp_size, 2, recur_cols), F32),
            pltpu.VMEM((1, recur_cols), F32),
            pltpu.VMEM((rows, query_cols), BF16),
            pltpu.VMEM((rows, out_width), F32),
            pltpu.VMEM((chunks, own_rows, chunk), BF16),
            pltpu.VMEM((chunks, own_rows, chunk), BF16),
            dma(19),
            dma(2),
            dma(sp_size),
            dma(sp_size),
            dma(2),
            dma(sp_size),
            dma(sp_size),
            dma(chunks),
            dma(chunks),
        ],
        compiler_params=pltpu.CompilerParams(collective_id=0, has_side_effects=True),
        name="layer",
    )(*operands)


def solution(mesh):
    in_specs = (
        P(("fs", "sp"), "tp"),
        P(),
        P(None, "tp"),
        P(None, "tp"),
        P("tp", None, None),
        P("tp", None, None),
        P("tp"),
        P(("fs", "sp"), "tp"),
        P(None, "tp"),
        P(None, "tp"),
        P(None, "tp"),
        P("tp"),
        P(),
        P("tp", None),
        P("tp", None),
        P(),
    )
    out_specs = P(("fs", "sp", "tp"), None)
    return jax.shard_map(
        functools.partial(body, mesh.shape["sp"], mesh.shape["tp"]),
        mesh=mesh, in_specs=in_specs, out_specs=out_specs, check_vma=False,
    )
```

time: 102 us -> 23.8 us (0.23)
  the two profiles are of different devices: /device:TPU:0 before, /device:TPU:29 now
where the time goes in v1:
time: 23.8 us; the launch traced here: 23.6 us
  Pallas kernels  20.5 us (86%)
  local copies, waits for them, and re-layouts  3.08 us (13%)
    pallas_call x1, Pallas kernels, body(): pl.pallas_call(functools.partial(kernel, sp_size, tp_size, conv_weight.sh...  20.5 us
    unnamed x2, local copies, waits for them, and re-layouts  3.08 us

profile of v1, /device:TPU:29, one launch (start us, length us, event | category | flops | bytes accessed | tf_op | source)
XLA Modules:
  0.0 23.6 jit_solution(18245777707335629478)
XLA Ops:
  0.0 1.4 %copy.17.extra_decay = f32[128,8]{1,0:T(8,128)} copy(f32[128,8]{0,1:T(8,128)} %param.23) | data formatting | bytes 8192 | tf_op args[7]
  1.4 20.5 %layer.1 = bf16[64,2048]{1,0:T(8,128)(2,1)} custom-call(bf16[128,1024]{1,0:T(8,128)(2,1)} %tokens.1, f32[1,2048]{1,0:T(1,128)} %bitcast.5, bf16[2048,512]{1,0:T(8,128)(2,1)} %w_recur_in.1, f32[4,512]{1,0:T(4,128)} %conv_weight.1, bf16[8,64,64]{2,1,0:T(8,128)(2,1)} %w_gate_decay.1, bf16[8,64,64]{2,1,0:T(8,128)(2,1)} %w_gate_input.1, f32[1,512]{1,0:T(1,128)} %bitcast.7, ...), custom_call_target="tpu_custom_call" | custom-call | tf_op jit(solution)/shard_map/layer/pallas_call | solution.py:428
  21.9 1.7 %copy.19 = bf16[64,2048]{1,0:T(8,128)(2,1)} copy(bf16[64,2048]{1,0:T(8,128)(2,1)} %layer.1) | data formatting | bytes 524288

commit v2 on v1

--- a/solution.py
+++ b/solution.py
@@ -125,14 +125,39 @@
 
     load("tok", tokens, tok.at[core])
     load("norm_gain", norm_gain, v_norm_gain)
+    load("r0", w_recur_in.at[mine], wr.at[mine])
     load("k0", w_key.at[mine], wkv.at[mine, pl.ds(0, key_cols)])
     load("v0", w_value.at[mine], wkv.at[mine, pl.ds(key_cols, wkv.shape[1] - key_cols)])
-    load("r0", w_recur_in.at[mine], wr.at[mine])
-    load("q0", w_query.at[mine], wq.at[mine])
+    load("r1", w_recur_in.at[theirs], wr.at[theirs])
     load("k1", w_key.at[theirs], wkv.at[theirs, pl.ds(0, key_cols)])
     load("v1", w_value.at[theirs], wkv.at[theirs, pl.ds(key_cols, wkv.shape[1] - key_cols)])
-    load("r1", w_recur_in.at[theirs], wr.at[theirs])
+
+    pl.semaphore_wait(barrier, sp_size)
+    plan["tok"].wait()
+    tok_copy = pltpu.make_async_remote_copy(
+        tok.at[core], tok.at[core], tok_sem.at[0], tok_sem.at[1],
+        device_id={"tp": partner}, device_id_type=MESH,
+    )
+    tok_copy.start()
+
+    def scale(part, columns):
+        wide = tok[part].astype(F32)
+        scaled[part] = (wide * v_norm_gain[:, columns]).astype(BF16)
+        return jnp.sum(wide * wide, axis=1, keepdims=True)
+
+    load("q0", w_query.at[mine], wq.at[mine])
     load("q1", w_query.at[theirs], wq.at[theirs])
+    plan["norm_gain"].wait()
+    squares = scale(core, mine)
+    own = scaled[core]
+    plan["r0"].wait()
+    acc_r[...] = dot(own, wr[mine, :])
+    plan["k0"].wait()
+    plan["v0"].wait()
+    acc_kv[...] = dot(own, wkv[mine, :])
+    plan["q0"].wait()
+    acc_q[...] = dot(own, wq[mine, :])
+
     load("gate_decay", w_gate_decay, v_gate_decay)
     load("gate_input", w_gate_input, v_gate_input)
     load("conv", conv_weight, v_conv)
@@ -142,57 +167,10 @@
     load("out_gain", out_gain, v_out_gain)
     load("wor", w_out_recur, wor)
     load("woa", w_out_attend, woa)
-
-    pl.semaphore_wait(barrier, sp_size)
-    tok_copy = pltpu.make_async_remote_copy(
-        tokens, tok.at[core], tok_sem.at[0], tok_sem.at[1],
-        device_id={"tp": partner}, device_id_type=MESH,
-    )
-    tok_copy.start()
-
-    def scale(part, columns):
-        wide = tok[part].astype(F32)
-        scaled[part] = (wide * v_norm_gain[:, columns]).astype(BF16)
-        return jnp.sum(wide * wide, axis=1, keepdims=True)
-
-    plan["tok"].wait()
-    plan["norm_gain"].wait()
-    squares = scale(core, mine)
-    own = scaled[core]
-    plan["k0"].wait()
-    plan["v0"].wait()
-    acc_kv[...] = dot(own, wkv[mine, :])
-    plan["r0"].wait()
-    acc_r[...] = dot(own, wr[mine, :])
-    plan["q0"].wait()
-    acc_q[...] = dot(own, wq[mine, :])
-
     tok_copy.wait_recv()
     squares = squares + scale(partner, theirs)
     inverse = lax.rsqrt(squares / width + norm_eps)
     far = scaled[partner]
-    plan["k1"].wait()
-    plan["v1"].wait()
-    kv[me] = ((acc_kv[...] + dot(far, wkv[theirs, :])) * inverse).astype(BF16)
-
-    def kv_copy(step):
-        return pltpu.make_async_remote_copy(
-            kv.at[me], kv.at[me], kv_send.at[step], kv_recv.at[step],
-            device_id={"sp": lax.rem(me + step, sp_size)}, device_id_type=MESH,
-        )
-
-    def kv_arrival(step):
-        slot = kv.at[me - step]
-        return pltpu.make_async_remote_copy(
-            slot, slot, kv_send.at[step], kv_recv.at[step],
-            device_id={"sp": lax.rem(me + step, sp_size)}, device_id_type=MESH,
-        )
-
-    for step in range(1, sp_size):
-        @pl.when(me + step < sp_size)
-        def _():
-            kv_copy(step).start()
-
     plan["r1"].wait()
     rbuf[pl.ds(halo, rows), :] = ((acc_r[...] + dot(far, wr[theirs, :])) * inverse).astype(BF16)
     halo_copy = pltpu.make_async_remote_copy(
@@ -207,6 +185,28 @@
     @pl.when(me == 0)
     def _():
         rbuf[pl.ds(0, halo), :] = jnp.zeros((halo, recur_cols), BF16)
+
+    plan["k1"].wait()
+    plan["v1"].wait()
+    kv[me] = ((acc_kv[...] + dot(far, wkv[theirs, :])) * inverse).astype(BF16)
+
+    def kv_copy(step):
+        return pltpu.make_async_remote_copy(
+            kv.at[me], kv.at[me], kv_send.at[step], kv_recv.at[step],
+            device_id={"sp": lax.rem(me + step, sp_size)}, device_id_type=MESH,
+        )
+
+    def kv_arrival(step):
+        slot = kv.at[me - step]
+        return pltpu.make_async_remote_copy(
+            slot, slot, kv_send.at[step], kv_recv.at[step],
+            device_id={"sp": lax.rem(me + step, sp_size)}, device_id_type=MESH,
+        )
+
+    for step in range(1, sp_size):
+        @pl.when(me + step < sp_size)
+        def _():
+            kv_copy(step).start()
 
     plan["q1"].wait()
     query = (acc_q[...] + dot(far, wq[theirs, :])) * (inverse * HEAD ** (-0.5))
@@ -269,6 +269,7 @@
         halo_copy.wait_recv()
 
     start = halo - (taps - 1)
+    spread = v_extra[...].T
     for p in range(pairs):
         columns = slice(p * PAIR, (p + 1) * PAIR)
         padded = rbuf[:, columns].astype(F32)
@@ -281,8 +282,8 @@
         input_gate = jax.nn.sigmoid(logits[:, PAIR:])
         extra = jnp.where(
             low,
-            jnp.broadcast_to(v_extra[:, 2 * p : 2 * p + 1], (rows, PAIR)),
-            jnp.broadcast_to(v_extra[:, 2 * p + 1 : 2 * p + 2], (rows, PAIR)),
+            jnp.broadcast_to(spread[:, 2 * p : 2 * p + 1], (rows, PAIR)),
+            jnp.broadcast_to(spread[:, 2 * p + 1 : 2 * p + 2], (rows, PAIR)),
         )
         log_decay = -lru_rate * decay_gate * v_base[:, columns] - extra
         decay = jnp.exp(log_decay)
@@ -418,7 +419,7 @@
     halo = 16
     line = lambda a: a.reshape(1, -1)
     operands = (tokens, line(norm_gain), w_recur_in, conv_weight, w_gate_decay, w_gate_input,
-                line(decay_base), extra_decay, w_query, w_key, w_value, line(mix_lambda),
+                line(decay_base), extra_decay.T, w_query, w_key, w_value, line(mix_lambda),
                 line(head_gain), w_out_recur, w_out_attend, line(out_gain))
     anywhere = pl.BlockSpec(memory_space=pl.ANY)
     specs = [anywhere] * len(operands)
@@ -427,7 +428,7 @@
     dma = lambda n: pltpu.SemaphoreType.DMA((n,))
     return pl.pallas_call(
         functools.partial(kernel, sp_size, tp_size, conv_weight.shape[0]),
-        out_shape=jax.ShapeDtypeStruct((own_rows, out_width), BF16),
+        out_shape=pltpu.VMEM((own_rows, out_width), BF16),
         in_specs=specs,
         out_specs=pl.BlockSpec(memory_space=pltpu.VMEM),
         scratch_shapes=[
@@ -443,7 +444,7 @@
             like(w_gate_decay),
             like(w_gate_input),
             like(operands[6]),
-            like(extra_decay),
+            like(operands[7]),
             like(operands[12]),
             like(operands[15]),
             pltpu.VMEM((pairs, PAIR, 2 * PAIR), BF16),

time: 23.8 us -> 18.7 us (0.79)
  Pallas kernels: 20.5 us -> 17.8 us
  local copies, waits for them, and re-layouts: 3.08 us -> 0.71 us
    pallas_call x1, Pallas kernels: 20.5 us -> 17.8 us  [body(): pl.pallas_call(functools.partial(kernel, sp_size, tp_size, conv_weight.sh...]
    unnamed x2 -> x1, local copies, waits for them, and re-layouts: 3.08 us -> 0.71 us
where the time goes in v2:
time: 18.7 us; the launch traced here: 18.5 us
  Pallas kernels  17.8 us (95%)
  local copies, waits for them, and re-layouts  0.71 us (4%)
    pallas_call x1, Pallas kernels, body(): pl.pallas_call(functools.partial(kernel, sp_size, tp_size, conv_weight.sh...  17.8 us
    unnamed x1, local copies, waits for them, and re-layouts  0.71 us

profile of v2, /device:TPU:29, one launch (start us, length us, event | category | flops | bytes accessed | tf_op | source)
XLA Modules:
  0.0 18.5 jit_solution(4337395164386804512)
XLA Ops:
  0.0 17.8 %layer.1 = bf16[64,2048]{1,0:T(8,128)(2,1)S(1)} custom-call(bf16[128,1024]{1,0:T(8,128)(2,1)} %tokens.1, f32[1,2048]{1,0:T(1,128)} %bitcast.6, bf16[2048,512]{1,0:T(8,128)(2,1)} %w_recur_in.1, f32[4,512]{1,0:T(4,128)} %conv_weight.1, bf16[8,64,64]{2,1,0:T(8,128)(2,1)} %w_gate_decay.1, bf16[8,64,64]{2,1,0:T(8,128)(2,1)} %w_gate_input.1, f32[1,512]{1,0:T(1,128)} %bitcast.9, ...), custom_call_target="tpu_custom_call" | custom-call | tf_op jit(solution)/shard_map/layer/pallas_call | solution.py:429
  17.8 0.7 %copy.18 = bf16[64,2048]{1,0:T(8,128)(2,1)} copy(bf16[64,2048]{1,0:T(8,128)(2,1)S(1)} %layer.1) | data formatting | bytes 524288

commit v3 on v2

--- a/solution.py
+++ b/solution.py
@@ -67,7 +67,6 @@
     gates,
     acc_kv,
     acc_r,
-    acc_q,
     kv,
     rbuf,
     qbuf,
@@ -81,6 +80,7 @@
     carried,
     attend_out,
     merged,
+    kept,
     part_out,
     part_in,
     load_sem,
@@ -155,8 +155,6 @@
     plan["k0"].wait()
     plan["v0"].wait()
     acc_kv[...] = dot(own, wkv[mine, :])
-    plan["q0"].wait()
-    acc_q[...] = dot(own, wq[mine, :])
 
     load("gate_decay", w_gate_decay, v_gate_decay)
     load("gate_input", w_gate_input, v_gate_input)
@@ -196,6 +194,18 @@
             device_id={"sp": lax.rem(me + step, sp_size)}, device_id_type=MESH,
         )
 
+    def direct(step):
+        return (me + step < sp_size) & ((me == 0) | (step != 2))
+
+    def relay():
+        slot = kv.at[me - 1]
+        return pltpu.make_async_remote_copy(
+            slot, slot, kv_send.at[0], kv_recv.at[2],
+            device_id={"sp": lax.rem(me + 1, sp_size)}, device_id_type=MESH,
+        )
+
+    relays = (me >= 2) & (me + 1 < sp_size)
+
     def kv_arrival(step):
         slot = kv.at[me - step]
         return pltpu.make_async_remote_copy(
@@ -204,12 +214,13 @@
         )
 
     for step in range(1, sp_size):
-        @pl.when(me + step < sp_size)
+        @pl.when(direct(step) & ((me > 0) | (step in (1, sp_size - 1))))
         def _():
             kv_copy(step).start()
 
+    plan["q0"].wait()
     plan["q1"].wait()
-    query = (acc_q[...] + dot(far, wq[theirs, :])) * (inverse * HEAD ** (-0.5))
+    query = (dot(own, wq[mine, :]) + dot(far, wq[theirs, :])) * (inverse * HEAD ** (-0.5))
     for h in range(heads):
         qbuf[h] = query[:, h * PAIR : (h + 1) * PAIR].astype(BF16)
 
@@ -247,7 +258,9 @@
                         attends[h, m] = attends[h, m] * fix + dot(expo.astype(BF16), value)
                     peaks[h, m] = peak
 
-    attend(me, True)
+    @pl.when(me > 0)
+    def _():
+        attend(me, True)
 
     plan["gate_decay"].wait()
     plan["gate_input"].wait()
@@ -320,12 +333,23 @@
         def _():
             carry_copy(step, me).start()
 
+    @pl.when(me == 0)
+    def _():
+        for step in range(2, sp_size - 1):
+            kv_copy(step).start()
+        attend(me, True)
+
     def one(step, unused):
         kv_arrival(step).wait_recv()
+
+        @pl.when(relays & (step == 1))
+        def _():
+            relay().start()
+
         attend(me - step, False)
         return unused
 
-    lax.fori_loop(1, me, one, 0)
+    lax.fori_loop(1, me, lambda k, unused: one(jnp.where(k == 1, 1, k + 1), unused), 0)
 
     carried[...] = jnp.zeros_like(carried)
 
@@ -342,7 +366,8 @@
         columns = slice(c * chunk, (c + 1) * chunk)
         merged[:, columns] = dot(recur_out, wor[:, columns])
 
-    lax.fori_loop(jnp.maximum(me, 1), me + 1, one, 0)
+    last = jnp.minimum(me, 2)
+    lax.fori_loop(jnp.maximum(last, 1), last + 1, one, 0)
 
     plan["head_gain"].wait()
     for h in range(heads):
@@ -366,26 +391,26 @@
             device_id={"tp": partner}, device_id_type=MESH,
         )
 
-    keep = pl.ds(pl.multiple_of(core * own_rows, own_rows), own_rows)
-    give = pl.ds(pl.multiple_of(partner * own_rows, own_rows), own_rows)
     for c in range(chunks):
         columns = slice(c * chunk, (c + 1) * chunk)
-        merged[:, columns] = merged[:, columns] + dot(attended, woa[:, columns])
-        part_out[c] = merged[give, columns].astype(BF16)
+        both = merged[:, columns] + dot(attended, woa[:, columns])
+        upper, lower = both[:own_rows], both[own_rows:]
+        part_out[c] = jnp.where(core == 0, lower, upper).astype(BF16)
         part_copy(c).start()
+        kept[:, columns] = jnp.where(core == 0, upper, lower)
 
     plan["out_gain"].wait()
     squares = jnp.zeros((own_rows, 1), F32)
     for c in range(chunks):
         columns = slice(c * chunk, (c + 1) * chunk)
         part_copy(c).wait_recv()
-        whole = merged[keep, columns] + part_in[c].astype(F32)
-        merged[keep, columns] = whole
+        whole = kept[:, columns] + part_in[c].astype(F32)
+        kept[:, columns] = whole
         squares = squares + jnp.sum(whole * whole, axis=1, keepdims=True)
     final = lax.rsqrt(squares / out.shape[1] + norm_eps)
     for c in range(chunks):
         columns = slice(c * chunk, (c + 1) * chunk)
-        out[:, columns] = (merged[keep, columns] * final * v_out_gain[:, columns]).astype(BF16)
+        out[:, columns] = (kept[:, columns] * final * v_out_gain[:, columns]).astype(BF16)
 
     tok_copy.wait_send()
     for c in range(chunks):
@@ -396,10 +421,17 @@
         halo_copy.wait_send()
 
     for step in range(1, sp_size):
+        @pl.when(direct(step))
+        def _():
+            kv_copy(step).wait_send()
+
         @pl.when(me + step < sp_size)
         def _():
-            kv_copy(step).wait_send()
             carry_copy(step, me).wait_send()
+
+    @pl.when(relays)
+    def _():
+        relay().wait_send()
 
 
 def body(sp_size, tp_size, *args):
@@ -450,7 +482,6 @@
             pltpu.VMEM((pairs, PAIR, 2 * PAIR), BF16),
             pltpu.VMEM((rows, kv_cols), F32),
             pltpu.VMEM((rows, recur_cols), F32),
-            pltpu.VMEM((rows, query_cols), F32),
             pltpu.VMEM((sp_size, rows, kv_cols), BF16),
             pltpu.VMEM((halo + rows, recur_cols), BF16),
             pltpu.VMEM((heads, rows, PAIR), BF16),
@@ -464,6 +495,7 @@
             pltpu.VMEM((1, recur_cols), F32),
             pltpu.VMEM((rows, query_cols), BF16),
             pltpu.VMEM((rows, out_width), F32),
+            pltpu.VMEM((own_rows, out_width), F32),
             pltpu.VMEM((chunks, own_rows, chunk), BF16),
             pltpu.VMEM((chunks, own_rows, chunk), BF16),
             dma(19),

time: 18.7 us -> 17.5 us (0.936)
  Pallas kernels: 17.8 us -> 16.6 us
    pallas_call x1, Pallas kernels: 17.8 us -> 16.6 us  [body(): pl.pallas_call(functools.partial(kernel, sp_size, tp_size, conv_weight.sh...]
where the time goes in v3:
time: 17.5 us; the launch traced here: 17.3 us
  Pallas kernels  16.6 us (95%)
  local copies, waits for them, and re-layouts  0.71 us (4%)
    pallas_call x1, Pallas kernels, body(): pl.pallas_call(functools.partial(kernel, sp_size, tp_size, conv_weight.sh...  16.6 us
    unnamed x1, local copies, waits for them, and re-layouts  0.71 us

profile of v3, /device:TPU:29, one launch (start us, length us, event | category | flops | bytes accessed | tf_op | source)
XLA Modules:
  0.0 17.3 jit_solution(11937085624366541385)
XLA Ops:
  0.0 16.6 %layer.1 = bf16[64,2048]{1,0:T(8,128)(2,1)S(1)} custom-call(bf16[128,1024]{1,0:T(8,128)(2,1)} %tokens.1, f32[1,2048]{1,0:T(1,128)} %bitcast.6, bf16[2048,512]{1,0:T(8,128)(2,1)} %w_recur_in.1, f32[4,512]{1,0:T(4,128)} %conv_weight.1, bf16[8,64,64]{2,1,0:T(8,128)(2,1)} %w_gate_decay.1, bf16[8,64,64]{2,1,0:T(8,128)(2,1)} %w_gate_input.1, f32[1,512]{1,0:T(1,128)} %bitcast.9, ...), custom_call_target="tpu_custom_call" | custom-call | tf_op jit(solution)/shard_map/layer/pallas_call | solution.py:461
  16.6 0.7 %copy.18 = bf16[64,2048]{1,0:T(8,128)(2,1)} copy(bf16[64,2048]{1,0:T(8,128)(2,1)S(1)} %layer.1) | data formatting | bytes 524288
